TPU v7x, 32 devices: a whole 2x2x4 slice. The times are simulated.
32 devices in a mesh: sp: 4 (over z), tp: 4 (over y, x), dp: 2 (over core).
Axes of the slice: x: 2, y: 2, z: 4, core: 2. Of those that a mesh axis runs over, the one named last changes fastest.
Arguments:
- latent: bfloat16 [2, 1024, 2048], P('dp', 'sp'), may hold values from -1.5 to 1.5
- condition: bfloat16 [2, 2048], P('dp', 'sp'), may hold values from -6 to 6
- context: bfloat16 [2, 1024, 2048], P('dp', 'sp'), may hold values from -6 to 6
- context_code: bfloat16 [2048], P('sp'), may hold values from -6 to 6
- shift_weight: bfloat16 [2048, 2048], P('sp', 'tp'), may hold values from -0.125 to 0.125
- scale_weight: bfloat16 [2048, 2048], P('sp', 'tp'), may hold values from -0.125 to 0.125
- gate_weight: bfloat16 [2048, 2048], P('sp', 'tp'), may hold values from -0.125 to 0.125
- norm_gain: float32 [2048], replicated, may hold values from 0.1 to 1.9
- query_weight: bfloat16 [2048, 1024], P(None, 'tp'), may hold values from -0.125 to 0.125
- key_weight: bfloat16 [2048, 256], P(None, 'tp'), may hold values from -0.125 to 0.125
- value_weight: bfloat16 [2048, 256], P(None, 'tp'), may hold values from -0.125 to 0.125
- output_weight: bfloat16 [1024, 2048], P('tp'), may hold values from -0.75 to 0.75
- query_gain: float32 [64], replicated, may hold values from 1 to 5.5
- key_gain: float32 [64], replicated, may hold values from 1 to 5.5
- context_bias: float32 [16], P('tp'), may hold values from 0.5 to 2
Outputs:
- updated: bfloat16 [2, 1024, 2048], P('dp', 'sp')
All inputs are finite; a program needn't handle non-finite values.
Results may differ from a plain program's by a relative error of at most 0.01405.
The roundings to bfloat16 on the way count: a program that leaves them out, or rounds other values in their place, can miss the bound.
Values may be sent and summed in bfloat16 or wider, within the bound.
No kernel may reach another device: no remote copies, remote signals or barrier semaphores. Data moves between devices by JAX's collectives and lax.ppermute only.
A program may use at most 64 MiB of HBM per device.

v0:
```python
import math

import jax
import jax.numpy as jnp
from jax import lax
from jax.sharding import PartitionSpec as P

GRID_W = 64


norm_eps = 1e-06
rope_base = 10000.0


def rotary_tables(position, grid_width, head_dim):
    grid_row = (position // grid_width).astype(jnp.float32)
    grid_col = (position % grid_width).astype(jnp.float32)
    quarter = head_dim // 4
    inverse = rope_base ** (-jnp.arange(quarter, dtype=jnp.float32) / quarter)
    angles = jnp.concatenate([grid_row[:, None] * inverse, grid_col[:, None] * inverse], axis=-1)
    return (jnp.cos(angles), jnp.sin(angles))


def head_norm(values, gain_row):
    return (
        values * lax.rsqrt(jnp.mean(values * values, axis=-1, keepdims=True) + norm_eps) * gain_row
    )


def rotate(values, cosine, sine_part):
    half_dim = values.shape[-1] // 2
    first_half = values[..., :half_dim]
    second_half = values[..., half_dim:]
    cos_rows = cosine[:, None, :]
    sin_rows = sine_part[:, None, :]
    return jnp.concatenate(
        [
            first_half * cos_rows - second_half * sin_rows,
            second_half * cos_rows + first_half * sin_rows,
        ],
        axis=-1,
    )


def modulated(tokens, gain_row, shift_row, scale_row):
    floats = tokens.astype(jnp.float32)
    normal = floats * lax.rsqrt(jnp.mean(floats * floats, axis=-1, keepdims=True) + norm_eps)
    return (normal * gain_row * (1.0 + scale_row) + shift_row).astype(jnp.bfloat16)


def on_device(
    latent,
    condition,
    context,
    context_code,
    shift_weight,
    scale_weight,
    gate_weight,
    norm_gain,
    query_weight,
    key_weight,
    value_weight,
    output_weight,
    query_gain,
    key_gain,
    context_bias,
):
    head_dim = query_gain.shape[0]
    tp_size = lax.axis_size("tp")
    activated = jax.nn.silu(condition[0].astype(jnp.float32)).astype(jnp.bfloat16)
    context_act = jax.nn.silu(context_code.astype(jnp.float32)).astype(jnp.bfloat16)
    partial_mod = jnp.stack(
        [
            jnp.dot(activated, shift_weight, preferred_element_type=jnp.float32),
            jnp.dot(activated, scale_weight, preferred_element_type=jnp.float32),
            jnp.dot(activated, gate_weight, preferred_element_type=jnp.float32),
            jnp.dot(context_act, shift_weight, preferred_element_type=jnp.float32),
            jnp.dot(context_act, scale_weight, preferred_element_type=jnp.float32),
        ]
    )
    summed = lax.psum(partial_mod, "sp")
    vectors = lax.all_gather(summed, "tp", axis=1, tiled=True)
    normed = modulated(latent[0], norm_gain, vectors[0], vectors[1])
    query_cols = query_weight.shape[1]
    key_cols = key_weight.shape[1]
    projected = jnp.concatenate(
        [
            jnp.dot(normed, query_weight, preferred_element_type=jnp.float32),
            jnp.dot(normed, key_weight, preferred_element_type=jnp.float32),
            jnp.dot(normed, value_weight, preferred_element_type=jnp.float32),
        ],
        axis=1,
    )
    seq_rows = projected.shape[0]
    position = lax.axis_index("sp") * seq_rows + jnp.arange(seq_rows, dtype=jnp.int32)
    cosine, sine_part = rotary_tables(position, GRID_W, head_dim)
    group_size = query_cols // head_dim
    queries = projected[:, :query_cols].reshape(seq_rows, group_size, head_dim)
    queries = rotate(head_norm(queries, query_gain), cosine, sine_part).astype(jnp.bfloat16)
    latent_keys = projected[:, query_cols : query_cols + key_cols].reshape(seq_rows, 1, head_dim)
    latent_keys = rotate(head_norm(latent_keys, key_gain), cosine, sine_part).astype(jnp.bfloat16)
    latent_values = projected[:, query_cols + key_cols :].astype(jnp.bfloat16)
    key_value = jnp.concatenate([latent_keys.reshape(seq_rows, head_dim), latent_values], axis=1)
    context_normed = modulated(context[0], norm_gain, vectors[3], vectors[4])
    context_keys = head_norm(
        jnp.dot(context_normed, key_weight, preferred_element_type=jnp.float32), key_gain
    )
    context_values = jnp.dot(context_normed, value_weight, preferred_element_type=jnp.float32)
    context_kv = lax.all_gather(
        jnp.concatenate(
            [context_keys.astype(jnp.bfloat16), context_values.astype(jnp.bfloat16)], axis=1
        ),
        "sp",
        axis=0,
        tiled=True,
    )
    score_scale = head_dim ** (-0.5)
    query_rows = queries.transpose(1, 0, 2).reshape(group_size * seq_rows, head_dim)
    bias_rows = jnp.repeat(context_bias, seq_rows)
    context_scores = jnp.dot(
        query_rows, context_kv[:, :head_dim].T, preferred_element_type=jnp.float32
    )
    context_scores = context_scores * score_scale + bias_rows[:, None]
    first_max = context_scores.max(axis=1)
    context_exp = jnp.exp(context_scores - first_max[:, None])
    start_state = (
        first_max,
        context_exp.sum(axis=1),
        jnp.dot(
            context_exp.astype(jnp.bfloat16),
            context_kv[:, head_dim:],
            preferred_element_type=jnp.float32,
        ),
    )
    arrived = lax.all_gather(key_value, "sp", axis=0, tiled=True)
    arrived_rows = arrived.shape[0]
    block_rows = math.gcd(arrived_rows, 1024)
    blocks = arrived.reshape(arrived_rows // block_rows, block_rows, 2 * head_dim)

    def absorb_block(state_now, pair_block):
        old_max, old_total, old_accum = state_now
        scores = (
            jnp.dot(query_rows, pair_block[:, :head_dim].T, preferred_element_type=jnp.float32)
            * score_scale
        )
        new_max = jnp.maximum(old_max, scores.max(axis=1))
        factor = jnp.exp(old_max - new_max)
        weights = jnp.exp(scores - new_max[:, None])
        new_accum = old_accum * factor[:, None] + jnp.dot(
            weights.astype(jnp.bfloat16),
            pair_block[:, head_dim:],
            preferred_element_type=jnp.float32,
        )
        return ((new_max, old_total * factor + weights.sum(axis=1), new_accum), None)

    final_state, unused = lax.scan(absorb_block, start_state, blocks)
    row_max, totals, accum = final_state
    attended = (accum / totals[:, None]).astype(jnp.bfloat16)
    attended = (
        attended.reshape(group_size, seq_rows, head_dim)
        .transpose(1, 0, 2)
        .reshape(seq_rows, query_cols)
    )
    own_rows = seq_rows // tp_size
    mixed = lax.psum_scatter(
        jnp.dot(attended, output_weight, preferred_element_type=jnp.float32).astype(jnp.bfloat16),
        "tp",
        scatter_dimension=0,
        tiled=True,
    ).astype(jnp.float32)
    own_latent = lax.dynamic_slice_in_dim(latent[0], lax.axis_index("tp") * own_rows, own_rows, 0)
    updated = (own_latent.astype(jnp.float32) + vectors[2] * mixed).astype(jnp.bfloat16)
    whole = lax.all_gather(updated, "tp", axis=0, tiled=True)
    return whole[None]


def solution(mesh):
    return jax.shard_map(
        on_device,
        mesh=mesh,
        in_specs=(
            P("dp", "sp", None),
            P("dp", "sp"),
            P("dp", "sp", None),
            P("sp"),
            P("sp", "tp"),
            P("sp", "tp"),
            P("sp", "tp"),
            P(),
            P(None, "tp"),
            P(None, "tp"),
            P(None, "tp"),
            P("tp", None),
            P(),
            P(),
            P("tp"),
        ),
        out_specs=P("dp", "sp", None),
        check_vma=False,
    )
```

profile of v0, /device:TPU:0, one launch (start us, length us, event | category | flops | bytes accessed | tf_op | source)
XLA Modules:
  0.0 148.6 jit_solution(14240642526981248333)
XLA Ops:
  6.6 0.8 fusion.67
  7.4 1.3 fusion.79
  8.7 1.2 fusion.78
  9.9 0.7 convert_element_type.122
  10.7 1.2 fusion.76
  11.9 1.2 fusion.75
  13.1 0.3 fusion.16
  13.5 0.3 fusion.7
  13.8 0.2 fusion.77
  14.0 20.5 %psum.7 = f32[5,512]{1,0:T(8,128)S(1)} all-reduce(f32[5,512]{1,0:T(8,128)S(1)} %stack.23), channel_id=1, replica_groups=mesh['sp'=4,'tp'=4,'dp'=2] {'sp'}, use_global_device_ids=true, to_apply=%region_0.1 | all-reduce | flops 2560 | bytes 20480 | tf_op jit(solution)/shard_map/psum | solution.py:81
  34.5 8.4 %all_gather.12 = f32[5,2048]{1,0:T(8,128)S(1)} all-gather(f32[5,512]{1,0:T(8,128)S(1)} %psum.7), channel_id=1, replica_groups=mesh['sp'=4,'tp'=4,'dp'=2] {'tp'}, dimensions={1}, use_global_device_ids=true | all-gather | bytes 51200 | tf_op jit(solution)/shard_map/all_gather | solution.py:82
  42.9 0.6 convolution_convert_fusion.2
  43.6 0.6 multiply_reduce_fusion.3
  44.2 0.3 copy-done.10
  44.5 0.6 convolution_convert_fusion.1
  45.2 0.6 multiply_reduce_fusion.2
  46.0 15.3 %all_gather.13 = bf16[1024,128]{0,1:T(8,128)(2,1)} all-gather(bf16[256,128]{0,1:T(8,128)(2,1)S(1)} %pad_maximum_fusion), channel_id=1, replica_groups=mesh['sp'=4,'tp'=4,'dp'=2] {'sp'}, dimensions={0}, use_global_device_ids=true | all-gather | bytes 327680 | tf_op jit(solution)/shard_map/all_gather | solution.py:109
  61.5 13.8 %all_gather.14 = bf16[1024,128]{0,1:T(8,128)(2,1)S(1)} all-gather(bf16[256,128]{0,1:T(8,128)(2,1)S(1)} %pad_maximum_fusion.1), channel_id=1, replica_groups=mesh['sp'=4,'tp'=4,'dp'=2] {'sp'}, dimensions={0}, use_global_device_ids=true | all-gather | bytes 327680 | tf_op jit(solution)/shard_map/all_gather | solution.py:135
  75.3 1.4 copy.17
  76.7 1.9 %multiply_reduce_fusion.1 = (f32[256,4]{0,1:T(4,128)S(1)}, f32[256,4,64]{0,2,1:T(8,128)S(1)}) fusion(bf16[4,64,2048]{2,1,0:T(8,128)(2,1)} %bitcast.98, bf16[1,256,2048]{2,1,0:T(8,128)(2,1)S(1)} %copy-done.1, f32[2048]{0:T(1024)S(1)} %bitcast.107, f32[2048]{0:T(1024)S(1)} %bitcast.110, f32[2048]{0:T(1024)S(1)} %copy-done.12, f32[256]{0:T(256)S(1)} %add_rsqrt_fusion.4), kind=kOutput, calls=%fused_computation.47 | convolution fusion | flops 271711232 | bytes 2388992 | tf_op jit(solution)/shard_map/dot_general | solution.py:88
  79.0 0.8 multiply_reduce_fusion
  79.8 0.2 copy-done.4
  80.0 0.8 fusion
  80.8 0.9 fusion.3
  81.6 0.7 fusion.1
  82.4 1.0 fusion.25
  83.3 0.8 fusion.34
  84.2 1.4 convolution_convert_fusion
  85.7 25.4 %reduce-scatter.2.cloned.1.call-done = bf16[64,2048]{1,0:T(8,128)(2,1)} async-done(((bf16[256,2048]{1,0:T(8,128)(2,1)}), bf16[64,2048]{1,0:T(8,128)(2,1)}) %reduce-scatter.2.cloned.1.call-update) | async-done | bytes 262160 | tf_op jit(solution)/shard_map/reduce_scatter | solution.py:165
  111.1 1.7 %fusion.44 = bf16[64,2048]{1,0:T(8,128)(2,1)} fusion(bf16[64,2048]{1,0:T(8,128)(2,1)} %reduce-scatter.2.cloned.1.call-done, f32[2048]{0:T(1024)S(1)} %bitcast.104, bf16[1,256,2048]{2,1,0:T(8,128)(2,1)S(1)} %copy-done.1, s32[]{:T(128)S(6)} %select_n.23), kind=kLoop, calls=%fused_computation.45 | loop fusion | flops 655360 | bytes 794628 | tf_op jit(solution)/shard_map/convert_element_type | solution.py:172
  112.8 26.7 %all-gather.2.cloned.1.call-done = bf16[256,2048]{1,0:T(8,128)(2,1)} async-done(((bf16[64,2048]{1,0:T(8,128)(2,1)}), bf16[256,2048]{1,0:T(8,128)(2,1)}) %all-gather.2.cloned.1.call-update) | async-done | bytes 1048592 | tf_op jit(solution)/shard_map/all_gather | solution.py:173
  139.5 2.3 %copy.26 = bf16[1,256,2048]{2,1,0:T(8,128)(2,1)} copy(bf16[1,256,2048]{2,1,0:T(8,128)(2,1)} %bitcast.97) | data formatting | bytes 2097152
  (54 shorter events, 1.0 us)
Async XLA Ops:
  6.5 77.6 %copy-start = (bf16[256,2048]{1,0:T(8,128)(2,1)S(1)}, bf16[256,2048]{1,0:T(8,128)(2,1)}, u32[]{:S(2)}) copy-start(bf16[256,2048]{1,0:T(8,128)(2,1)} %param.26) | copy-start | bytes 3145732
  6.5 6.6 %copy-start.2 = (bf16[1,256,2048]{2,1,0:T(8,128)(2,1)S(1)}, bf16[1,256,2048]{2,1,0:T(8,128)(2,1)}, u32[]{:S(2)}) copy-start(bf16[1,256,2048]{2,1,0:T(8,128)(2,1)} %param.17) | copy-start | bytes 3145732
  6.5 6.9 %copy-start.1 = (bf16[1,256,2048]{2,1,0:T(8,128)(2,1)S(1)}, bf16[1,256,2048]{2,1,0:T(8,128)(2,1)}, u32[]{:S(2)}) copy-start(bf16[1,256,2048]{2,1,0:T(8,128)(2,1)} %param.15) | copy-start | bytes 3145732
  6.5 104.5 %reduce-scatter.2.cloned.1.call-start = ((), (), s32[]{:S(2)}) async-start(), calls=%async_computation.1 | async-start | bytes 1310720 | tf_op jit(solution)/shard_map/reduce_scatter | solution.py:165
  7.4 6.3 %copy-start.5 = (bf16[512,512]{1,0:T(8,128)(2,1)S(1)}, bf16[512,512]{1,0:T(8,128)(2,1)}, u32[]{:S(2)}) copy-start(bf16[512,512]{1,0:T(8,128)(2,1)} %param.21) | copy-start | bytes 1572868
  9.9 33.0 %copy-start.9 = (bf16[2048,64]{0,1:T(8,128)(2,1)S(1)}, bf16[2048,64]{0,1:T(8,128)(2,1)}, u32[]{:S(2)}) copy-start(bf16[2048,64]{0,1:T(8,128)(2,1)} %param.25) | copy-start | bytes 786436
  9.9 33.0 %copy-start.12 = (f32[2048]{0:T(1024)S(1)}, f32[2048]{0:T(1024)}, u32[]{:S(2)}) copy-start(f32[2048]{0:T(1024)} %param.22) | copy-start | bytes 24580
  34.5 9.1 %copy-start.11 = (bf16[2048,64]{0,1:T(8,128)(2,1)S(1)}, bf16[2048,64]{0,1:T(8,128)(2,1)}, u32[]{:S(2)}) copy-start(bf16[2048,64]{0,1:T(8,128)(2,1)} %param.24) | copy-start | bytes 786436
  43.5 1.0 copy-start.10
  45.1 0.7 copy-start.8
  45.1 0.8 copy-start.6
  45.1 30.2 %copy-start.3 = (bf16[2048,256]{1,0:T(8,128)(2,1)S(1)}, bf16[2048,256]{1,0:T(8,128)(2,1)}, u32[]{:S(2)}) copy-start(bf16[2048,256]{1,0:T(8,128)(2,1)} %param.23) | copy-start | bytes 3145732
  76.7 2.1 %copy-start.7 = (f32[64]{0:T(128)S(1)}, f32[64]{0:T(128)}, u32[]{:S(2)}) copy-start(f32[64]{0:T(128)} %param.27) | copy-start | bytes 772
  79.0 1.0 copy-start.4
  85.6 53.8 %all-gather.2.cloned.1.call-start = ((), (), s32[]{:S(2)}) async-start(), calls=%async_computation.2 | async-start | bytes 1310720 | tf_op jit(solution)/shard_map/all_gather | solution.py:173
Sparse Core Ops, SparseCore 0:
  85.8 25.2 reduce-scatter.1
  113.0 26.4 all-gather.1
where the time goes:
time: 149 us
  blocking collectives  57.9 us (39%)
  waiting for transfers between devices  52.1 us (35%)
  matrix products  14.3 us (10%)
  between operations  13.7 us (9%)
  other arithmetic  6.16 us (4%)
  local copies, waits for them, and re-layouts  4.4 us (3%)
    all_gather x1, waiting for transfers between devices, on_device(): whole = lax.all_gather(updated, 'tp', axis=0, tiled=True)  26.7 us
    reduce_scatter x1, waiting for transfers between devices, on_device(): lax.psum_scatter(jnp.dot(attended, output_weight, preferred_element_type=...  25.4 us
    psum x1, blocking collectives, on_device(): summed = lax.psum(partial_mod, 'sp')  20.5 us
    all_gather x1, blocking collectives, on_device(): lax.all_gather(jnp.concatenate([context_keys.astype(jnp.bfloat16), contex...  15.3 us
    all_gather x1, blocking collectives, on_device(): arrived = lax.all_gather(key_value, 'sp', axis=0, tiled=True)  13.8 us
    all_gather x1, blocking collectives, on_device(): vectors = lax.all_gather(summed, 'tp', axis=1, tiled=True)  8.36 us
    unnamed x30, local copies, waits for them, and re-layouts  4.33 us
  transfers between devices with their start and end apart: 2, of which 2 were waited for; matrix products, arithmetic and copies ran while one was open for 0% of the time, Pallas kernels for 0%

commit v1 on v0

v1 whole, which is shorter than its diff:
```python
import functools
import math

import jax
import jax.numpy as jnp
from jax import lax
from jax.experimental import pallas as pl
from jax.experimental.pallas import tpu as pltpu
from jax.sharding import PartitionSpec as P


GRID_W = 64
DIRECT_LIMIT = 4
KERNEL_VMEM = 20 << 20

norm_eps = 1e-06
rope_base = 10000.0

VMEM = pl.BlockSpec(memory_space=pltpu.VMEM)
SMEM = pl.BlockSpec(memory_space=pltpu.SMEM)
HBM = pl.BlockSpec(memory_space=pltpu.HBM)


def dot(left, right):
    return jnp.dot(left, right, preferred_element_type=jnp.float32)


def dot_t(left, right):
    return lax.dot_general(
        left, right, (((1,), (1,)), ((), ())), preferred_element_type=jnp.float32
    )


def call(kernel, outs, specs, flops, *args, **kwargs):
    return pl.pallas_call(
        kernel,
        out_shape=outs,
        in_specs=specs,
        out_specs=jax.tree.map(lambda _: VMEM, outs),
        cost_estimate=pl.CostEstimate(flops=flops, bytes_accessed=0, transcendentals=0),
        compiler_params=pltpu.CompilerParams(vmem_limit_bytes=KERNEL_VMEM),
        **kwargs,
    )(*args)


def modulation_kernel(*refs):
    sources, out_ref, buffers, semaphores = refs[:5], refs[5], refs[6:11], refs[11]
    copies = [
        pltpu.make_async_copy(source, buffer, semaphores.at[i])
        for i, (source, buffer) in enumerate(zip(sources, buffers))
    ]
    for copy in copies:
        copy.start()
    copies[0].wait()
    copies[1].wait()
    row = lax.broadcasted_iota(jnp.int32, (16, buffers[0].shape[1]), 0)
    rows = jnp.where(row == 0, buffers[0][...].astype(jnp.float32), 0.0)
    rows = jnp.where(row == 1, buffers[1][...].astype(jnp.float32)[None], rows)
    rows = (rows / (1.0 + jnp.exp(-rows))).astype(jnp.bfloat16)
    for i, copy in enumerate(copies[2:]):
        copy.wait()
        out_ref[2 * i : 2 * i + 2, :] = dot(rows, buffers[2 + i][...])[:2]


def normal_kernel(context_hbm, latent_hbm, context_ref, latent_ref, context_out, latent_out, semaphores):
    steps = []
    for source, buffer, out_ref in (
        (context_hbm, context_ref, context_out),
        (latent_hbm, latent_ref, latent_out),
    ):
        block = math.gcd(source.shape[0], 64)
        for start in range(0, source.shape[0], block):
            part = pl.ds(start, block)
            copy = pltpu.make_async_copy(
                source.at[part], buffer.at[part], semaphores.at[len(steps)]
            )
            steps.append((copy, buffer, out_ref, part))
    for copy, _, _, _ in steps:
        copy.start()
    for copy, buffer, out_ref, part in steps:
        copy.wait()
        floats = buffer[part].astype(jnp.float32)
        mean = jnp.mean(floats * floats, axis=-1, keepdims=True)
        out_ref[part] = lax.rsqrt(mean + norm_eps)


def head_norm(values, gain_row):
    mean = jnp.mean(values * values, axis=-1, keepdims=True)
    return values * lax.rsqrt(mean + norm_eps) * gain_row


def rotate(values, cosine, sine_part):
    half_dim = values.shape[-1] // 2
    turned = jnp.concatenate([-values[:, half_dim:], values[:, :half_dim]], axis=1)
    return values * cosine + turned * sine_part


def key_value_kernel(
    index_ref,
    pieces_ref,
    latent_ref,
    context_ref,
    latent_factor_ref,
    context_factor_ref,
    norm_gain_ref,
    key_w_ref,
    value_w_ref,
    gain_ref,
    cos_ref,
    sin_ref,
    kv_ref,
    normed_ref,
    gate_ref,
    rows_ref,
):
    me = index_ref[0]
    count = pieces_ref.shape[0]
    width = pieces_ref.shape[2]
    for mask in range(count):
        start = pl.multiple_of((me ^ mask) * width, width)
        rows_ref[:, pl.ds(start, width)] = pieces_ref[mask]
    ctx_rows = context_ref.shape[0]
    for is_latent, in_ref, factor_ref in (
        (False, context_ref, context_factor_ref),
        (True, latent_ref, latent_factor_ref),
    ):
        row = 0 if is_latent else 1
        shift, scale = rows_ref[row : row + 1, :], rows_ref[row + 2 : row + 3, :]
        scale = norm_gain_ref[...] * (1.0 + scale)
        normed = in_ref[...].astype(jnp.float32) * factor_ref[...]
        normed = (normed * scale + shift).astype(jnp.bfloat16)
        keys = head_norm(dot_t(normed, key_w_ref[...]), gain_ref[...])
        if is_latent:
            normed_ref[...] = normed
            keys = rotate(keys, cos_ref[...], sin_ref[...])
        values = dot_t(normed, value_w_ref[...])
        part = slice(ctx_rows, None) if is_latent else slice(0, ctx_rows)
        kv_ref[part, :] = jnp.concatenate([keys, values], axis=1).astype(jnp.bfloat16)
    gate_ref[...] = rows_ref[4:5, :]


def query_kernel(scale, normed_ref, weight_ref, gain_ref, cos_ref, sin_ref, out_ref):
    all_heads = dot(normed_ref[...], weight_ref[...])
    head_dim = gain_ref.shape[1]
    rows = all_heads.shape[0]
    for head in range(all_heads.shape[1] // head_dim):
        values = all_heads[:, head * head_dim : (head + 1) * head_dim]
        values = rotate(head_norm(values, gain_ref[...]), cos_ref[...], sin_ref[...])
        values = values.astype(jnp.bfloat16) * scale
        out_ref[head * rows : (head + 1) * rows, :] = jnp.concatenate(
            [values, jnp.zeros_like(values)], axis=1
        ).astype(jnp.bfloat16)


def with_ones(pairs):
    lane = lax.broadcasted_iota(jnp.int32, pairs.shape, 1)
    return jnp.where(lane < pairs.shape[1] // 2, jnp.ones_like(pairs), pairs)


def block_scores(queries, pair_refs, bias, ctx_rows):
    context = [dot_t(queries, ref[:ctx_rows, :]) for ref in pair_refs]
    latent = [dot_t(queries, ref[ctx_rows:, :]) for ref in pair_refs]
    tops = [functools.reduce(jnp.maximum, kind).max(axis=1, keepdims=True) for kind in (context, latent)]
    return context, latent, jnp.maximum(tops[0] + bias, tops[1])


def weigh(context, latent, top, bias, pair_refs, ctx_rows):
    weights = [jnp.exp(values - (top - bias)).astype(jnp.bfloat16) for values in context]
    weights += [jnp.exp(values - top).astype(jnp.bfloat16) for values in latent]
    pairs = [ref[:ctx_rows, :] for ref in pair_refs] + [ref[ctx_rows:, :] for ref in pair_refs]
    pairs = with_ones(jnp.concatenate(pairs, axis=0))
    return dot(jnp.concatenate(weights, axis=1), pairs)


def attend_own_kernel(ctx_rows, bias_ref, query_ref, *refs):
    pair_refs, (top_ref, sum_ref) = refs[:-2], refs[-2:]
    heads = bias_ref.shape[0]
    rows = query_ref.shape[0] // heads
    for head in range(heads):
        part = slice(head * rows, (head + 1) * rows)
        bias = bias_ref[head]
        context, latent, top = block_scores(query_ref[part, :], pair_refs, bias, ctx_rows)
        top_ref[part, :] = top
        sum_ref[part, :] = weigh(context, latent, top, bias, pair_refs, ctx_rows)


def attend_rest_kernel(ctx_rows, bias_ref, query_ref, top_ref, sum_ref, *refs):
    pair_refs, out_ref = refs[:-1], refs[-1]
    heads = bias_ref.shape[0]
    rows = query_ref.shape[0] // heads
    head_dim = query_ref.shape[1] // 2
    for head in range(heads):
        part = slice(head * rows, (head + 1) * rows)
        bias = bias_ref[head]
        context, latent, top = block_scores(query_ref[part, :], pair_refs, bias, ctx_rows)
        old_top = top_ref[part, :]
        top = jnp.maximum(top, old_top)
        total = sum_ref[part, :] * jnp.exp(old_top - top)
        total = total + weigh(context, latent, top, bias, pair_refs, ctx_rows)
        out_ref[:, head * head_dim : (head + 1) * head_dim] = (
            total[:, head_dim:] / total[:, :head_dim]
        ).astype(jnp.bfloat16)


def own_partial_kernel(heads_ref, weight_ref, out_ref):
    out_ref[...] = dot(heads_ref[...], weight_ref[...]).astype(jnp.bfloat16)


def output_kernel(
    index_ref, own_ref, one_ref, two_ref, three_ref, latent_ref, gate_ref, *refs
):
    weight_refs, out_ref = refs[:-1], refs[-1]
    width = out_ref.shape[1]
    columns = pl.ds(pl.multiple_of(pl.program_id(0) * width, width), width)
    core = index_ref[1]

    def project(x_ref, y_ref, first_ref, second_ref):
        diagonal = jnp.concatenate([first_ref[:, columns], second_ref[:, columns]], axis=0)
        parts = [
            dot(heads_ref[...], rows).astype(jnp.bfloat16).astype(jnp.float32)
            for heads_ref, rows in (
                (one_ref, x_ref[:, columns]),
                (two_ref, y_ref[:, columns]),
                (three_ref, diagonal),
            )
        ]
        mixed = (own_ref[:, columns].astype(jnp.float32) + parts[0]) + (parts[1] + parts[2])
        out_ref[...] = (
            latent_ref[:, columns].astype(jnp.float32) + gate_ref[:, columns] * mixed
        ).astype(jnp.bfloat16)

    near_ref, far_ref, other_near_ref, other_far_ref = weight_refs

    @pl.when(core == 0)
    def _():
        project(near_ref, other_near_ref, far_ref, other_far_ref)

    @pl.when(core != 0)
    def _():
        project(other_near_ref, near_ref, other_far_ref, far_ref)


def direct(size):
    return size <= DIRECT_LIMIT and size & (size - 1) == 0


def swap(values, axis, mask):
    size = lax.axis_size(axis)
    return lax.ppermute(values, axis, [(i, i ^ mask) for i in range(size)])


def core_swap(values, axis, masks):
    size, cores = lax.axis_size(axis), len(masks)
    pairs = [
        (i * cores + core, (i ^ mask) * cores + core)
        for i in range(size)
        for core, mask in enumerate(masks)
    ]
    return lax.ppermute(values, (axis, "dp"), pairs)


def exchange(values, axis):
    masks = range(1, lax.axis_size(axis))
    return [values] + [swap(values, axis, mask) for mask in masks]


def paired_sum(parts):
    while len(parts) > 1:
        parts = [parts[i] + parts[i + 1] for i in range(0, len(parts), 2)]
    return parts[0]


def on_device(
    latent,
    condition,
    context,
    context_code,
    shift_weight,
    scale_weight,
    gate_weight,
    norm_gain,
    query_weight,
    key_weight,
    value_weight,
    output_weight,
    query_gain,
    key_gain,
    context_bias,
):
    head_dim = query_gain.shape[0]
    sp_size = lax.axis_size("sp")
    bf16, f32 = jnp.bfloat16, jnp.float32
    shape = jax.ShapeDtypeStruct
    latent, context = latent[0], context[0]
    seq_rows, width = latent.shape
    ctx_rows = context.shape[0]
    core = lax.axis_index("dp")
    index = jnp.stack([lax.axis_index("tp"), core]).astype(jnp.int32)
    gain_row, key_row, query_row = norm_gain[None], key_gain[None], query_gain[None]

    cols = shift_weight.shape[1]
    sources = [condition, context_code, shift_weight, scale_weight, gate_weight]
    partial_mod = call(
        modulation_kernel,
        pltpu.VMEM((8, cols), f32),
        [HBM] * 5,
        2**20,
        *(pltpu.with_memory_space_constraint(source, pltpu.HBM) for source in sources),
        scratch_shapes=[pltpu.VMEM(source.shape, bf16) for source in sources]
        + [pltpu.SemaphoreType.DMA((5,))],
    )
    blocks = sum(rows // math.gcd(rows, 64) for rows in (ctx_rows, seq_rows))
    context_tokens, latent_tokens, context_factor, latent_factor = call(
        normal_kernel,
        [
            pltpu.VMEM((ctx_rows, width), bf16),
            pltpu.VMEM((seq_rows, width), bf16),
            pltpu.VMEM((ctx_rows, 1), f32),
            pltpu.VMEM((seq_rows, 1), f32),
        ],
        [HBM] * 2,
        2**24,
        *(pltpu.with_memory_space_constraint(tokens, pltpu.HBM) for tokens in (context, latent)),
        scratch_shapes=[pltpu.SemaphoreType.DMA((blocks,))],
    )
    if direct(sp_size):
        summed = paired_sum(exchange(partial_mod, "sp"))
    else:
        summed = lax.psum(partial_mod, "sp")
    pieces = jnp.stack(exchange(summed, "tp"))

    near = core_swap(output_weight, "tp", (1, 2))
    half = output_weight.shape[0] // 2
    passed = lax.dynamic_slice_in_dim(near, core * half, half, 0)
    far = core_swap(passed, "tp", (2, 1))
    gathered = [near, far, swap(near, "dp", 1), swap(far, "dp", 1)]

    position = lax.axis_index("sp") * seq_rows + jnp.arange(seq_rows, dtype=jnp.int32)
    grid_row = (position // GRID_W).astype(f32)
    grid_col = (position % GRID_W).astype(f32)
    inverse = rope_base ** (-jnp.arange(head_dim // 4, dtype=f32) / (head_dim // 4))
    angles = jnp.concatenate([grid_row[:, None] * inverse, grid_col[:, None] * inverse], axis=-1)
    angles = jnp.concatenate([angles, angles], axis=-1)
    cosine, sine_part = jnp.cos(angles), jnp.sin(angles)

    own_kv, normed, gate_row = call(
        key_value_kernel,
        [
            shape((ctx_rows + seq_rows, 2 * head_dim), bf16),
            shape((seq_rows, width), bf16),
            shape((1, width), f32),
        ],
        [SMEM] + [VMEM] * 11,
        2**28,
        index,
        pieces,
        latent_tokens,
        context_tokens,
        latent_factor,
        context_factor,
        gain_row,
        key_weight.T,
        value_weight.T,
        key_row,
        cosine,
        sine_part,
        scratch_shapes=[pltpu.VMEM((8, width), f32)],
    )
    if direct(sp_size):
        pairs = exchange(own_kv, "sp")
    query_cols = query_weight.shape[1]
    heads = query_cols // head_dim
    score_scale = head_dim ** (-0.5)
    queries = call(
        functools.partial(query_kernel, score_scale),
        shape((heads * seq_rows, 2 * head_dim), bf16),
        [VMEM] * 5,
        2**28,
        normed,
        query_weight,
        query_row,
        cosine,
        sine_part,
    )
    if direct(sp_size):
        top_score, sums = call(
            functools.partial(attend_own_kernel, ctx_rows),
            [shape((heads * seq_rows, 1), f32), shape((heads * seq_rows, 2 * head_dim), f32)],
            [SMEM] + [VMEM] * 2,
            2**28,
            context_bias,
            queries,
            own_kv,
        )
        attended = call(
            functools.partial(attend_rest_kernel, ctx_rows),
            shape((seq_rows, query_cols), bf16),
            [SMEM] + [VMEM] * (2 + len(pairs)),
            2**30,
            context_bias,
            queries,
            top_score,
            sums,
            *pairs[1:],
        )
    else:
        attended = scanned_attention(own_kv, ctx_rows, queries, context_bias, head_dim, heads)

    heads_of = exchange(attended, "tp")
    own_partial = call(
        own_partial_kernel,
        shape((seq_rows, width), bf16),
        [VMEM] * 2,
        2**28,
        attended,
        output_weight,
    )
    block = math.gcd(width, 512)
    updated = pl.pallas_call(
        output_kernel,
        grid=(width // block,),
        out_shape=shape((seq_rows, width), bf16),
        in_specs=[SMEM] + [VMEM] * (6 + len(gathered)),
        out_specs=pl.BlockSpec((seq_rows, block), lambda i: (0, i)),
        cost_estimate=pl.CostEstimate(flops=2**30, bytes_accessed=0, transcendentals=0),
        name="output",
        compiler_params=pltpu.CompilerParams(vmem_limit_bytes=KERNEL_VMEM),
    )(index, own_partial, *heads_of[1:], latent, gate_row, *gathered)
    return updated[None]


def scanned_attention(own_kv, ctx_rows, queries, context_bias, head_dim, heads):
    contexts = lax.all_gather(own_kv[:ctx_rows], "sp", axis=0, tiled=True)
    arrived = lax.all_gather(own_kv[ctx_rows:], "sp", axis=0, tiled=True)
    query_rows = queries[:, :head_dim]
    seq_rows = query_rows.shape[0] // heads
    bias_rows = jnp.repeat(context_bias, seq_rows)
    scores = dot(query_rows, contexts[:, :head_dim].T) + bias_rows[:, None]
    first_max = scores.max(axis=1)
    weights = jnp.exp(scores - first_max[:, None])
    start = (
        first_max,
        weights.sum(axis=1),
        dot(weights.astype(jnp.bfloat16), contexts[:, head_dim:]),
    )
    block_rows = math.gcd(arrived.shape[0], 1024)
    blocks = arrived.reshape(-1, block_rows, 2 * head_dim)

    def absorb_block(state_now, pair_block):
        old_max, old_total, old_accum = state_now
        scores = dot(query_rows, pair_block[:, :head_dim].T)
        new_max = jnp.maximum(old_max, scores.max(axis=1))
        factor = jnp.exp(old_max - new_max)
        weights = jnp.exp(scores - new_max[:, None])
        new_accum = old_accum * factor[:, None] + dot(
            weights.astype(jnp.bfloat16), pair_block[:, head_dim:]
        )
        return ((new_max, old_total * factor + weights.sum(axis=1), new_accum), None)

    (row_max, totals, accum), unused = lax.scan(absorb_block, start, blocks)
    attended = (accum / totals[:, None]).astype(jnp.bfloat16)
    attended = attended.reshape(heads, seq_rows, head_dim).transpose(1, 0, 2)
    return attended.reshape(seq_rows, heads * head_dim)


def solution(mesh):
    return jax.shard_map(
        on_device,
        mesh=mesh,
        in_specs=(
            P("dp", "sp", None),
            P("dp", "sp"),
            P("dp", "sp", None),
            P("sp"),
            P("sp", "tp"),
            P("sp", "tp"),
            P("sp", "tp"),
            P(),
            P(None, "tp"),
            P(None, "tp"),
            P(None, "tp"),
            P("tp", None),
            P(),
            P(),
            P("tp"),
        ),
        out_specs=P("dp", "sp", None),
        check_vma=False,
    )
```

time: 149 us -> 62.2 us (0.42)
  blocking collectives: 57.9 us -> 0 us
  waiting for transfers between devices: 52.1 us -> 19.9 us
  starting transfers between devices: 0.04 us -> 21.4 us
  Pallas kernels: 0 us -> 18.2 us
  matrix products: 14.3 us -> 0 us
  between operations: 13.7 us -> 0.22 us
  other arithmetic: 6.16 us -> 0.8 us
  local copies, waits for them, and re-layouts: 4.4 us -> 1.38 us
    all_gather x3 -> x0, blocking collectives: 37.4 us -> none  [the longest x1 15.3 us: on_device(): lax.all_gather(jnp.concatenate([context_keys.astype(jnp.bfloat16), contex...]
    all_gather x1 -> x0, waiting for transfers between devices: 26.7 us -> none  [on_device(): whole = lax.all_gather(updated, 'tp', axis=0, tiled=True)]
    reduce_scatter x1 -> x0, waiting for transfers between devices: 25.4 us -> none  [on_device(): lax.psum_scatter(jnp.dot(attended, output_weight, preferred_element_type=...]
    ppermute x0 -> x16, starting transfers between devices: none -> 21.4 us  [the longest x14 16.3 us: swap(): return lax.ppermute(values, axis, [(i, i ^ mask) for i in range(size)])]
    psum x1 -> x0, blocking collectives: 20.5 us -> none  [on_device(): summed = lax.psum(partial_mod, 'sp')]
    ppermute x0 -> x16, waiting for transfers between devices: none -> 19.9 us  [the longest x2 10.2 us: core_swap(): return lax.ppermute(values, (axis, 'dp'), pairs)]
    pallas_call x0 -> x8, Pallas kernels: none -> 18.2 us  [the longest x7 14.8 us: call(): pl.pallas_call(kernel, out_shape=outs, in_specs=specs, out_specs=jax.tree...]
    dot_general x15 -> x0, matrix products: 14.3 us -> none  [the longest x1 1.94 us: on_device(): jnp.dot(normed, query_weight, preferred_element_type=jnp.float32)]
  transfers between devices with their start and end apart: 2 -> 16, of which waited for: 2 -> 6; matrix products, arithmetic and copies ran while one was open for 0% -> 1% of each run, Pallas kernels for 0% -> 24%
where the time goes in v1:
time: 62.2 us; the launch traced here: 61.8 us
  starting transfers between devices  21.4 us (34%)
  waiting for transfers between devices  19.9 us (32%)
  Pallas kernels  18.2 us (29%)
  local copies, waits for them, and re-layouts  1.38 us (2%)
  other arithmetic  0.8 us (1%)
    ppermute x14, starting transfers between devices, swap(): return lax.ppermute(values, axis, [(i, i ^ mask) for i in range(size)])  16.3 us
    pallas_call x7, Pallas kernels, call(): pl.pallas_call(kernel, out_shape=outs, in_specs=specs, out_specs=jax.tree...  14.8 us
    ppermute x2, waiting for transfers between devices, core_swap(): return lax.ppermute(values, (axis, 'dp'), pairs)  10.2 us
    ppermute x14, waiting for transfers between devices, swap(): return lax.ppermute(values, axis, [(i, i ^ mask) for i in range(size)])  9.65 us
    ppermute x2, starting transfers between devices, core_swap(): return lax.ppermute(values, (axis, 'dp'), pairs)  5.08 us
    pallas_call x1, Pallas kernels, on_device(): pl.pallas_call(output_kernel, grid=(width // block,), out_shape=shape((se...  3.41 us
    unnamed x18, local copies, waits for them, and re-layouts  1.34 us
  transfers between devices with their start and end apart: 16, of which 6 were waited for; matrix products, arithmetic and copies ran while one was open for 1% of the time, Pallas kernels for 24%

profile of v1, /device:TPU:0, one launch (start us, length us, event | category | flops | bytes accessed | tf_op | source)
XLA Modules:
  0.0 61.8 jit_solution(9869986795721970772)
XLA Ops:
  0.0 3.0 %collective-permute-start.12 = (bf16[256,2048]{1,0:T(8,128)(2,1)}, bf16[256,2048]{1,0:T(8,128)(2,1)S(1)}, u32[]{:S(2)}, u32[]{:S(2)}) collective-permute-start(bf16[256,2048]{1,0:T(8,128)(2,1)} %weight_ref.3), channel_id=1, source_target_pairs={{0,2},{1,5},{2,0},{3,7},{4,6},{5,1},{6,4},{7,3},{8,10},{9,13},{10,... | collective-permute-start | bytes 3145736 | tf_op jit(solution)/shard_map/ppermute | solution.py:259
  3.0 1.7 %shard_map.145 = f32[8,512]{1,0:T(8,128)S(1)} custom-call(bf16[1,512]{1,0:T(2,128)(2,1)} %refs_0_.1, bf16[512]{0:T(512)(128)(2,1)} %refs_1_.1, bf16[512,512]{1,0:T(8,128)(2,1)} %refs_2_.1, bf16[512,512]{1,0:T(8,128)(2,1)} %refs_3_.1, bf16[512,512]{1,0:T(8,128)(2,1)} %refs_4_.1), custom_call_target="tpu_custom_call" | custom-call | flops 1048576 | tf_op jit(solution)/shard_map/pallas_call | solution.py:35
  4.6 1.6 %collective-permute-start = (f32[8,512]{1,0:T(8,128)S(1)}, f32[8,512]{1,0:T(8,128)S(1)}, u32[]{:S(2)}, u32[]{:S(2)}) collective-permute-start(f32[8,512]{1,0:T(8,128)S(1)} %shard_map.145), channel_id=1, source_target_pairs={{0,8},{8,0},{16,24},{24,16},{1,9},{9,1},{17,25},{25,17},{2,10},{10... | collective-permute-start | bytes 49160 | tf_op jit(solution)/shard_map/ppermute | solution.py:249
  6.3 2.6 %collective-permute-start.1 = (f32[8,512]{1,0:T(8,128)S(1)}, f32[8,512]{1,0:T(8,128)S(1)}, u32[]{:S(2)}, u32[]{:S(2)}) collective-permute-start(f32[8,512]{1,0:T(8,128)S(1)} %shard_map.145), channel_id=1, source_target_pairs={{0,16},{8,24},{16,0},{24,8},{1,17},{9,25},{17,1},{25,9},{2,18},{10... | collective-permute-start | bytes 49160 | tf_op jit(solution)/shard_map/ppermute | solution.py:249
  8.9 0.2 collective-permute-start.2
  9.1 6.8 %collective-permute-done.12.refs_0_ = bf16[256,2048]{1,0:T(8,128)(2,1)S(1)} collective-permute-done((bf16[256,2048]{1,0:T(8,128)(2,1)}, bf16[256,2048]{1,0:T(8,128)(2,1)S(1)}, u32[]{:S(2)}, u32[]{:S(2)}) %collective-permute-start.12) | collective-permute-done | bytes 1048608 | tf_op jit(solution)/shard_map/ppermute | solution.py:259
  16.0 2.1 %collective-permute-start.13 = (bf16[128,2048]{1,0:T(8,128)(2,1)S(1)}, bf16[128,2048]{1,0:T(8,128)(2,1)S(1)}, u32[]{:S(2)}, u32[]{:S(2)}) collective-permute-start(bf16[128,2048]{1,0:T(8,128)(2,1)S(1)} %constant_dynamic-slice_fusion), channel_id=1, source_target_pairs={{0,4},{1,3},{2,6},{3,1},{4,0},{5,7},{6,2},{7,5},{8,12},{9,11},{10,... | collective-permute-start | bytes 1572872 | tf_op jit(solution)/shard_map/ppermute | solution.py:259
  18.1 0.1 broadcast_multiply_fusion.1
  18.2 0.6 fusion
  18.9 1.6 %collective-permute-start.3 = (f32[8,512]{1,0:T(8,128)S(1)}, f32[8,512]{1,0:T(8,128)S(1)}, u32[]{:S(2)}, u32[]{:S(2)}) collective-permute-start(f32[8,512]{1,0:T(8,128)S(1)} %add_add_fusion), channel_id=1, source_target_pairs={{0,2},{2,0},{4,6},{6,4},{1,3},{3,1},{5,7},{7,5},{8,10},{10,8},{12,... | collective-permute-start | bytes 49160 | tf_op jit(solution)/shard_map/ppermute | solution.py:249
  20.4 0.5 collective-permute-start.4
  20.9 1.5 %collective-permute-start.5 = (f32[8,512]{1,0:T(8,128)S(1)}, f32[8,512]{1,0:T(8,128)S(1)}, u32[]{:S(2)}, u32[]{:S(2)}) collective-permute-start(f32[8,512]{1,0:T(8,128)S(1)} %add_add_fusion), channel_id=1, source_target_pairs={{0,6},{2,4},{4,2},{6,0},{1,7},{3,5},{5,3},{7,1},{8,14},{10,12},{12... | collective-permute-start | bytes 49160 | tf_op jit(solution)/shard_map/ppermute | solution.py:249
  22.4 3.4 %collective-permute-done.13.refs_1_ = bf16[128,2048]{1,0:T(8,128)(2,1)S(1)} collective-permute-done((bf16[128,2048]{1,0:T(8,128)(2,1)S(1)}, bf16[128,2048]{1,0:T(8,128)(2,1)S(1)}, u32[]{:S(2)}, u32[]{:S(2)}) %collective-permute-start.13) | collective-permute-done | bytes 524320 | tf_op jit(solution)/shard_map/ppermute | solution.py:259
  25.8 0.1 pad_add_fusion.index_ref
  25.9 2.2 %shard_map.146 = (bf16[256,2048]{1,0:T(8,128)(2,1)S(1)}, bf16[256,2048]{1,0:T(8,128)(2,1)S(1)}, f32[256,1]{1,0:T(8,128)S(1)}, f32[256,1]{1,0:T(8,128)S(1)}) custom-call(bf16[256,2048]{1,0:T(8,128)(2,1)} %bitcast.21, bf16[256,2048]{1,0:T(8,128)(2,1)} %bitcast.14), custom_call_target="tpu_custom_call" | custom-call | flops 16777216 | tf_op jit(solution)/shard_map/pallas_call | solution.py:35
  28.2 0.7 %copy-done.5 = f32[2048]{0:T(1024)S(1)} copy-done((f32[2048]{0:T(1024)S(1)}, f32[2048]{0:T(1024)}, u32[]{:S(2)}) %copy-start.5) | copy-done | bytes 8216
  28.9 2.2 %shard_map.147 = (bf16[512,128]{1,0:T(8,128)(2,1)S(1)}, bf16[256,2048]{1,0:T(8,128)(2,1)S(1)}, f32[1,2048]{1,0:T(1,128)S(1)}) custom-call(s32[2]{0:T(128)S(1)} %pad_add_fusion.index_ref, f32[4,8,512]{2,1,0:T(8,128)S(1)} %pad_maximum_fusion.1.pieces_ref, bf16[256,2048]{1,0:T(8,128)(2,1)S(1)} %get-tuple-element.14.latent_ref, ...), custom_call_target="tpu_custom_call" | custom-call | flops 268435456 | tf_op jit(solution)/shard_map/pallas_call | solution.py:35
  31.1 2.1 %collective-permute-start.6 = (bf16[512,128]{1,0:T(8,128)(2,1)S(1)}, bf16[512,128]{1,0:T(8,128)(2,1)S(1)}, u32[]{:S(2)}, u32[]{:S(2)}) collective-permute-start(bf16[512,128]{1,0:T(8,128)(2,1)S(1)} %get-tuple-element.19.refs_0_), channel_id=1, source_target_pairs={{0,8},{8,0},{16,24},{24,16},{1,9},{9,1},{17,25},{25,17},{2,10},{10... | collective-permute-start | bytes 393224 | tf_op jit(solution)/shard_map/ppermute | solution.py:249
  33.2 2.6 %collective-permute-start.7 = (bf16[512,128]{1,0:T(8,128)(2,1)S(1)}, bf16[512,128]{1,0:T(8,128)(2,1)S(1)}, u32[]{:S(2)}, u32[]{:S(2)}) collective-permute-start(bf16[512,128]{1,0:T(8,128)(2,1)S(1)} %get-tuple-element.19.refs_0_), channel_id=1, source_target_pairs={{0,16},{8,24},{16,0},{24,8},{1,17},{9,25},{17,1},{25,9},{2,18},{10... | collective-permute-start | bytes 393224 | tf_op jit(solution)/shard_map/ppermute | solution.py:249
  35.8 0.7 %copy-done.7 = f32[64]{0:T(128)S(1)} copy-done((f32[64]{0:T(128)S(1)}, f32[64]{0:T(128)}, u32[]{:S(2)}) %copy-start.7) | copy-done | bytes 280
  36.5 2.4 %shard_map.148.query_ref = bf16[1024,128]{1,0:T(8,128)(2,1)S(1)} custom-call(bf16[256,2048]{1,0:T(8,128)(2,1)S(1)} %get-tuple-element.18.normed_ref, bf16[2048,256]{1,0:T(8,128)(2,1)S(1)} %copy-done.1, f32[1,64]{1,0:T(1,128)S(1)} %bitcast.20, f32[256,64]{1,0:T(8,128)S(1)} %get-tuple-element.24.cos_ref, f32[256,64]{1,0:T(8,128)S(1)} %get-tuple-element.23.sin_ref), custom_call_target="tpu_custom_call" | custom-call | flops 268435456 | tf_op jit(solution)/shard_map/pallas_call | solution.py:35
  38.9 1.9 %shard_map.149 = (f32[1024,1]{1,0:T(8,128)S(1)}, f32[1024,128]{1,0:T(8,128)S(1)}) custom-call(f32[4]{0:T(128)S(1)} %copy-done.8, bf16[1024,128]{1,0:T(8,128)(2,1)S(1)} %shard_map.148.query_ref, bf16[512,128]{1,0:T(8,128)(2,1)S(1)} %get-tuple-element.19.refs_0_), custom_call_target="tpu_custom_call" | custom-call | flops 268435456 | tf_op jit(solution)/shard_map/pallas_call | solution.py:35
  40.8 5.3 %collective-permute-done.7.refs_1_ = bf16[512,128]{1,0:T(8,128)(2,1)S(1)} collective-permute-done((bf16[512,128]{1,0:T(8,128)(2,1)S(1)}, bf16[512,128]{1,0:T(8,128)(2,1)S(1)}, u32[]{:S(2)}, u32[]{:S(2)}) %collective-permute-start.7) | collective-permute-done | bytes 131104 | tf_op jit(solution)/shard_map/ppermute | solution.py:249
  46.1 3.9 %shard_map.150.heads_ref = bf16[256,256]{1,0:T(8,128)(2,1)S(1)} custom-call(f32[4]{0:T(128)S(1)} %copy-done.8, bf16[1024,128]{1,0:T(8,128)(2,1)S(1)} %shard_map.148.query_ref, f32[1024,1]{1,0:T(8,128)S(1)} %get-tuple-element.20.top_ref, f32[1024,128]{1,0:T(8,128)S(1)} %get-tuple-element.21.sum_ref, bf16[512,128]{1,0:T(8,128)(2,1)S(1)} %collective-permute-done.6.refs_0_, ...), custom_call_target="tpu_custom_call" | custom-call | flops 1073741824 | tf_op jit(solution)/shard_map/pallas_call | solution.py:35
  50.0 1.6 %collective-permute-start.10 = (bf16[256,256]{1,0:T(8,128)(2,1)S(1)}, bf16[256,256]{1,0:T(8,128)(2,1)S(1)}, u32[]{:S(2)}, u32[]{:S(2)}) collective-permute-start(bf16[256,256]{1,0:T(8,128)(2,1)S(1)} %shard_map.150.heads_ref), channel_id=1, source_target_pairs={{0,4},{2,6},{4,0},{6,2},{1,5},{3,7},{5,1},{7,3},{8,12},{10,14},{12... | collective-permute-start | bytes 393224 | tf_op jit(solution)/shard_map/ppermute | solution.py:249
  51.6 1.5 %collective-permute-start.11 = (bf16[256,256]{1,0:T(8,128)(2,1)S(1)}, bf16[256,256]{1,0:T(8,128)(2,1)S(1)}, u32[]{:S(2)}, u32[]{:S(2)}) collective-permute-start(bf16[256,256]{1,0:T(8,128)(2,1)S(1)} %shard_map.150.heads_ref), channel_id=1, source_target_pairs={{0,6},{2,4},{4,2},{6,0},{1,7},{3,5},{5,3},{7,1},{8,14},{10,12},{12... | collective-permute-start | bytes 393224 | tf_op jit(solution)/shard_map/ppermute | solution.py:249
  53.1 0.5 collective-permute-start.9
  53.6 0.4 shard_map.151.own_ref
  54.0 2.8 %collective-permute-done.10.two_ref = bf16[256,256]{1,0:T(8,128)(2,1)S(1)} collective-permute-done((bf16[256,256]{1,0:T(8,128)(2,1)S(1)}, bf16[256,256]{1,0:T(8,128)(2,1)S(1)}, u32[]{:S(2)}, u32[]{:S(2)}) %collective-permute-start.10) | collective-permute-done | bytes 131104 | tf_op jit(solution)/shard_map/ppermute | solution.py:249
  56.8 1.0 %collective-permute-done.11.three_ref = bf16[256,256]{1,0:T(8,128)(2,1)S(1)} collective-permute-done((bf16[256,256]{1,0:T(8,128)(2,1)S(1)}, bf16[256,256]{1,0:T(8,128)(2,1)S(1)}, u32[]{:S(2)}, u32[]{:S(2)}) %collective-permute-start.11) | collective-permute-done | bytes 131104 | tf_op jit(solution)/shard_map/ppermute | solution.py:249
  57.8 0.5 collective-permute-done.9.one_ref
  58.4 3.4 %output.1 = bf16[256,2048]{1,0:T(8,128)(2,1)} custom-call(s32[2]{0:T(128)S(1)} %pad_add_fusion.index_ref, bf16[256,2048]{1,0:T(8,128)(2,1)S(1)} %shard_map.151.own_ref, bf16[256,256]{1,0:T(8,128)(2,1)S(1)} %collective-permute-done.9.one_ref, bf16[256,256]{1,0:T(8,128)(2,1)S(1)} %collective-permute-done.10.two_ref, ...), custom_call_target="tpu_custom_call" | custom-call | flops 1073741824 | tf_op jit(solution)/shard_map/output/pallas_call | solution.py:419
  (34 shorter events, 0.1 us)
Async XLA Ops:
  0.0 16.0 %collective-permute-start.12 = (bf16[256,2048]{1,0:T(8,128)(2,1)}, bf16[256,2048]{1,0:T(8,128)(2,1)S(1)}, u32[]{:S(2)}, u32[]{:S(2)}) collective-permute-start(bf16[256,2048]{1,0:T(8,128)(2,1)} %weight_ref.3), channel_id=1, source_target_pairs={{0,2},{1,5},{2,0},{3,7},{4,6},{5,1},{6,4},{7,3},{8,10},{9,13},{10,... | collective-permute-start | bytes 3145736 | tf_op jit(solution)/shard_map/ppermute | solution.py:259
  4.6 14.2 %collective-permute-start = (f32[8,512]{1,0:T(8,128)S(1)}, f32[8,512]{1,0:T(8,128)S(1)}, u32[]{:S(2)}, u32[]{:S(2)}) collective-permute-start(f32[8,512]{1,0:T(8,128)S(1)} %shard_map.145), channel_id=1, source_target_pairs={{0,8},{8,0},{16,24},{24,16},{1,9},{9,1},{17,25},{25,17},{2,10},{10... | collective-permute-start | bytes 49160 | tf_op jit(solution)/shard_map/ppermute | solution.py:249
  6.3 12.5 %collective-permute-start.1 = (f32[8,512]{1,0:T(8,128)S(1)}, f32[8,512]{1,0:T(8,128)S(1)}, u32[]{:S(2)}, u32[]{:S(2)}) collective-permute-start(f32[8,512]{1,0:T(8,128)S(1)} %shard_map.145), channel_id=1, source_target_pairs={{0,16},{8,24},{16,0},{24,8},{1,17},{9,25},{17,1},{25,9},{2,18},{10... | collective-permute-start | bytes 49160 | tf_op jit(solution)/shard_map/ppermute | solution.py:249
  8.9 10.0 %collective-permute-start.2 = (f32[8,512]{1,0:T(8,128)S(1)}, f32[8,512]{1,0:T(8,128)S(1)}, u32[]{:S(2)}, u32[]{:S(2)}) collective-permute-start(f32[8,512]{1,0:T(8,128)S(1)} %shard_map.145), channel_id=1, source_target_pairs={{0,24},{8,16},{16,8},{24,0},{1,25},{9,17},{17,9},{25,1},{2,26},{10... | collective-permute-start | bytes 49160 | tf_op jit(solution)/shard_map/ppermute | solution.py:249
  16.0 9.8 %collective-permute-start.13 = (bf16[128,2048]{1,0:T(8,128)(2,1)S(1)}, bf16[128,2048]{1,0:T(8,128)(2,1)S(1)}, u32[]{:S(2)}, u32[]{:S(2)}) collective-permute-start(bf16[128,2048]{1,0:T(8,128)(2,1)S(1)} %constant_dynamic-slice_fusion), channel_id=1, source_target_pairs={{0,4},{1,3},{2,6},{3,1},{4,0},{5,7},{6,2},{7,5},{8,12},{9,11},{10,... | collective-permute-start | bytes 1572872 | tf_op jit(solution)/shard_map/ppermute | solution.py:259
  18.1 40.3 %collective-permute-start.14 = (bf16[256,2048]{1,0:T(8,128)(2,1)S(1)}, bf16[256,2048]{1,0:T(8,128)(2,1)S(1)}, u32[]{:S(2)}, u32[]{:S(2)}) collective-permute-start(bf16[256,2048]{1,0:T(8,128)(2,1)S(1)} %collective-permute-done.12.refs_0_), channel_id=1, source_target_pairs={{0,1},{1,0},{2,3},{3,2},{4,5},{5,4},{6,7},{7,6},{8,9},{9,8},{10,11... | collective-permute-start | bytes 3145736 | tf_op jit(solution)/shard_map/ppermute | solution.py:249
  18.9 9.2 %collective-permute-start.3 = (f32[8,512]{1,0:T(8,128)S(1)}, f32[8,512]{1,0:T(8,128)S(1)}, u32[]{:S(2)}, u32[]{:S(2)}) collective-permute-start(f32[8,512]{1,0:T(8,128)S(1)} %add_add_fusion), channel_id=1, source_target_pairs={{0,2},{2,0},{4,6},{6,4},{1,3},{3,1},{5,7},{7,5},{8,10},{10,8},{12,... | collective-permute-start | bytes 49160 | tf_op jit(solution)/shard_map/ppermute | solution.py:249
  20.4 7.7 %collective-permute-start.4 = (f32[8,512]{1,0:T(8,128)S(1)}, f32[8,512]{1,0:T(8,128)S(1)}, u32[]{:S(2)}, u32[]{:S(2)}) collective-permute-start(f32[8,512]{1,0:T(8,128)S(1)} %add_add_fusion), channel_id=1, source_target_pairs={{0,4},{2,6},{4,0},{6,2},{1,5},{3,7},{5,1},{7,3},{8,12},{10,14},{12... | collective-permute-start | bytes 49160 | tf_op jit(solution)/shard_map/ppermute | solution.py:249
  20.9 7.2 %collective-permute-start.5 = (f32[8,512]{1,0:T(8,128)S(1)}, f32[8,512]{1,0:T(8,128)S(1)}, u32[]{:S(2)}, u32[]{:S(2)}) collective-permute-start(f32[8,512]{1,0:T(8,128)S(1)} %add_add_fusion), channel_id=1, source_target_pairs={{0,6},{2,4},{4,2},{6,0},{1,7},{3,5},{5,3},{7,1},{8,14},{10,12},{12... | collective-permute-start | bytes 49160 | tf_op jit(solution)/shard_map/ppermute | solution.py:249
  25.8 32.6 %collective-permute-start.15 = (bf16[128,2048]{1,0:T(8,128)(2,1)S(1)}, bf16[128,2048]{1,0:T(8,128)(2,1)S(1)}, u32[]{:S(2)}, u32[]{:S(2)}) collective-permute-start(bf16[128,2048]{1,0:T(8,128)(2,1)S(1)} %collective-permute-done.13.refs_1_), channel_id=1, source_target_pairs={{0,1},{1,0},{2,3},{3,2},{4,5},{5,4},{6,7},{7,6},{8,9},{9,8},{10,11... | collective-permute-start | bytes 1572872 | tf_op jit(solution)/shard_map/ppermute | solution.py:249
  25.9 2.3 %copy-start.3 = (bf16[2048,64]{0,1:T(8,128)(2,1)S(1)}, bf16[2048,64]{0,1:T(8,128)(2,1)}, u32[]{:S(2)}) copy-start(bf16[2048,64]{0,1:T(8,128)(2,1)} %param.24) | copy-start | bytes 786436
  25.9 2.3 %copy-start.4 = (bf16[2048,64]{0,1:T(8,128)(2,1)S(1)}, bf16[2048,64]{0,1:T(8,128)(2,1)}, u32[]{:S(2)}) copy-start(bf16[2048,64]{0,1:T(8,128)(2,1)} %param.25) | copy-start | bytes 786436
  28.2 0.7 %copy-start.5 = (f32[2048]{0:T(1024)S(1)}, f32[2048]{0:T(1024)}, u32[]{:S(2)}) copy-start(f32[2048]{0:T(1024)} %param.22) | copy-start | bytes 24580
  28.2 0.7 %copy-start.6 = (f32[64]{0:T(128)S(1)}, f32[64]{0:T(128)}, u32[]{:S(2)}) copy-start(f32[64]{0:T(128)} %param.28) | copy-start | bytes 772
  28.9 7.0 %copy-start.1 = (bf16[2048,256]{1,0:T(8,128)(2,1)S(1)}, bf16[2048,256]{1,0:T(8,128)(2,1)}, u32[]{:S(2)}) copy-start(bf16[2048,256]{1,0:T(8,128)(2,1)} %weight_ref.2) | copy-start | bytes 3145732
  31.1 9.8 %collective-permute-start.6 = (bf16[512,128]{1,0:T(8,128)(2,1)S(1)}, bf16[512,128]{1,0:T(8,128)(2,1)S(1)}, u32[]{:S(2)}, u32[]{:S(2)}) collective-permute-start(bf16[512,128]{1,0:T(8,128)(2,1)S(1)} %get-tuple-element.19.refs_0_), channel_id=1, source_target_pairs={{0,8},{8,0},{16,24},{24,16},{1,9},{9,1},{17,25},{25,17},{2,10},{10... | collective-permute-start | bytes 393224 | tf_op jit(solution)/shard_map/ppermute | solution.py:249
  33.2 12.9 %collective-permute-start.7 = (bf16[512,128]{1,0:T(8,128)(2,1)S(1)}, bf16[512,128]{1,0:T(8,128)(2,1)S(1)}, u32[]{:S(2)}, u32[]{:S(2)}) collective-permute-start(bf16[512,128]{1,0:T(8,128)(2,1)S(1)} %get-tuple-element.19.refs_0_), channel_id=1, source_target_pairs={{0,16},{8,24},{16,0},{24,8},{1,17},{9,25},{17,1},{25,9},{2,18},{10... | collective-permute-start | bytes 393224 | tf_op jit(solution)/shard_map/ppermute | solution.py:249
  35.8 10.3 %collective-permute-start.8 = (bf16[512,128]{1,0:T(8,128)(2,1)S(1)}, bf16[512,128]{1,0:T(8,128)(2,1)S(1)}, u32[]{:S(2)}, u32[]{:S(2)}) collective-permute-start(bf16[512,128]{1,0:T(8,128)(2,1)S(1)} %get-tuple-element.19.refs_0_), channel_id=1, source_target_pairs={{0,24},{8,16},{16,8},{24,0},{1,25},{9,17},{17,9},{25,1},{2,26},{10... | collective-permute-start | bytes 393224 | tf_op jit(solution)/shard_map/ppermute | solution.py:249
  35.8 0.7 %copy-start.7 = (f32[64]{0:T(128)S(1)}, f32[64]{0:T(128)}, u32[]{:S(2)}) copy-start(f32[64]{0:T(128)} %param.27) | copy-start | bytes 772
  36.5 2.4 %copy-start.8 = (f32[4]{0:T(128)S(1)}, f32[4]{0:T(128)}, u32[]{:S(2)}) copy-start(f32[4]{0:T(128)} %bias_ref.3) | copy-start | bytes 52
  46.1 7.4 %copy-start.2 = (bf16[256,2048]{1,0:T(8,128)(2,1)S(1)}, bf16[256,2048]{1,0:T(8,128)(2,1)}, u32[]{:S(2)}) copy-start(bf16[256,2048]{1,0:T(8,128)(2,1)} %weight_ref.3) | copy-start | bytes 3145732
  50.0 8.4 %copy-start = (bf16[1,256,2048]{2,1,0:T(8,128)(2,1)S(1)}, bf16[1,256,2048]{2,1,0:T(8,128)(2,1)}, u32[]{:S(2)}) copy-start(bf16[1,256,2048]{2,1,0:T(8,128)(2,1)} %param.15) | copy-start | bytes 3145732
  50.0 6.8 %collective-permute-start.10 = (bf16[256,256]{1,0:T(8,128)(2,1)S(1)}, bf16[256,256]{1,0:T(8,128)(2,1)S(1)}, u32[]{:S(2)}, u32[]{:S(2)}) collective-permute-start(bf16[256,256]{1,0:T(8,128)(2,1)S(1)} %shard_map.150.heads_ref), channel_id=1, source_target_pairs={{0,4},{2,6},{4,0},{6,2},{1,5},{3,7},{5,1},{7,3},{8,12},{10,14},{12... | collective-permute-start | bytes 393224 | tf_op jit(solution)/shard_map/ppermute | solution.py:249
  51.6 6.2 %collective-permute-start.11 = (bf16[256,256]{1,0:T(8,128)(2,1)S(1)}, bf16[256,256]{1,0:T(8,128)(2,1)S(1)}, u32[]{:S(2)}, u32[]{:S(2)}) collective-permute-start(bf16[256,256]{1,0:T(8,128)(2,1)S(1)} %shard_map.150.heads_ref), channel_id=1, source_target_pairs={{0,6},{2,4},{4,2},{6,0},{1,7},{3,5},{5,3},{7,1},{8,14},{10,12},{12... | collective-permute-start | bytes 393224 | tf_op jit(solution)/shard_map/ppermute | solution.py:249
  53.1 5.3 %collective-permute-start.9 = (bf16[256,256]{1,0:T(8,128)(2,1)S(1)}, bf16[256,256]{1,0:T(8,128)(2,1)S(1)}, u32[]{:S(2)}, u32[]{:S(2)}) collective-permute-start(bf16[256,256]{1,0:T(8,128)(2,1)S(1)} %shard_map.150.heads_ref), channel_id=1, source_target_pairs={{0,2},{2,0},{4,6},{6,4},{1,3},{3,1},{5,7},{7,5},{8,10},{10,8},{12,... | collective-permute-start | bytes 393224 | tf_op jit(solution)/shard_map/ppermute | solution.py:249
